TPU v7x, 32 devices: a whole 2x2x4 slice. The times are simulated.
32 devices in a mesh: ep: 4 (over y, x), tp: 8 (over z, core).
Axes of the slice: x: 2, y: 2, z: 4, core: 2. Of those that a mesh axis runs over, the one named last changes fastest.
Arguments:
- query_rows: bfloat16 [512, 2048], P('ep', 'tp'), may hold values from -32 to 32
- key_rows: bfloat16 [512, 2048], P('ep', 'tp'), may hold values from -8 to 8
- value_rows: bfloat16 [512, 2048], P('ep', 'tp'), may hold values from -8 to 8
- query_norm_gain: float32 [64], replicated, may hold values from 0.1 to 1.9
- key_gain: float32 [64], replicated, may hold values from 0.1 to 1.9
- break_offset: float32 [32], P('tp'), may hold values from -12 to 3
- mixer_out_weight: bfloat16 [2048, 2048], P('tp'), may hold values from -0.75 to 0.75
- routed_tokens: bfloat16 [4096, 2048], P(('ep', 'tp')), may hold values from -6 to 6
- expert_gain: float32 [2048], replicated, may hold values from 0.1 to 1.9
- routes: int32 [4096, 2], P(('ep', 'tp')), may hold values from 0 to 3, as said below
- route_scores: float32 [4096, 2], P(('ep', 'tp')), may hold values from -6 to 6
- gate_weight: bfloat16 [4, 2048, 3584], P('ep', None, 'tp'), may hold values from -0.125 to 0.125
- up_weight: bfloat16 [4, 2048, 3584], P('ep', None, 'tp'), may hold values from -0.125 to 0.125
- down_weight: bfloat16 [4, 3584, 2048], P('ep', 'tp'), may hold values from -0.09375 to 0.09375
Outputs:
- attention_output: bfloat16 [512, 2048], P(('ep', 'tp'))
- expert_output: bfloat16 [4096, 2048], P(('ep', 'tp'))
Inputs may be any that keep to these rules, and one draw needn't show every extreme that they name: `routes`: each row names 2 different experts. Among the rows of one device no expert is named more than 64 times, and one expert is named exactly 64 times by the rows of every device.
All inputs are finite; a program needn't handle non-finite values.
Results may differ from a plain program's by a relative error of at most 0.018.
Values may be sent and summed in bfloat16 or wider, within the bound.
A program may use at most 128 MiB of HBM per device.

v0:
```python
import functools

import jax
import jax.numpy as jnp
from jax import lax
from jax.experimental import pallas as pl
from jax.experimental.pallas import tpu as pltpu
from jax.sharding import PartitionSpec as P

HEAD_DIM = 64
TOP_K = 2
EPS = 1e-06
TAGS = 128
MESH = pl.DeviceIdType.MESH
F32, BF16 = jnp.float32, jnp.bfloat16

EARLY_SHARE = 96
A_CHUNKS = 4
B_CHUNKS = 2


def dot(a, b):
    return jnp.dot(a, b, preferred_element_type=F32)


def dot_t(a, b):
    return lax.dot_general(a, b, (((1,), (1,)), ((), ())), preferred_element_type=F32)


def split3(x):
    high = x.astype(BF16)
    rest = x - high.astype(F32)
    mid = rest.astype(BF16)
    low = (rest - mid.astype(F32)).astype(BF16)
    return high, mid, low


def rcopy(src, dst, send, recv, dev):
    return pltpu.make_async_remote_copy(
        src_ref=src, dst_ref=dst, send_sem=send, recv_sem=recv, device_id=dev, device_id_type=MESH
    )


def norm_heads(ref, gain):
    out = []
    for start in range(0, ref.shape[1], HEAD_DIM):
        x = ref[:, start : start + HEAD_DIM].astype(F32)
        x = x * lax.rsqrt(jnp.mean(x * x, axis=1, keepdims=True) + EPS)
        out.append((x * gain).astype(BF16))
    return out


def body(
    experts, levels, count, wide, early,
    query, key, value, query_gain, key_gain, offset, mixer, tokens, expert_gain, routes, scores,
    gate, up, down,
    att_out, exp_out,
    wg, wu, wd, wm, normed, xb, xa, xbs, oa, ob, pa, pb, qb, qa, wh, wl,
    ral, rah, mb, rbl, rbh, fa, acc, kv, hm, hmo, ms, rml, rmh,
    lw_sem, pw_send, pw_recv, hm_sem,
    pa_send, pa_recv, kv_send, kv_recv, pb_send, pb_recv, rb_send, rb_recv, ra_send, ra_recv,
    fb_up, fb_dn, fb_recv, fa_up, fa_dn, fa_recv,
    za_send, za_low, za_high, zb_send, zb_low, zb_high, zm_send, zm_low, zm_high,
):
    E, Z, C = experts, levels, count
    A, B = early, wide - early
    slots = TOP_K * C
    cap = slots // E
    R = slots // A_CHUNKS
    TB = C // B_CHUNKS
    ep = lax.axis_index("ep")
    tp = lax.axis_index("tp")
    z = tp // 2
    core = tp % 2
    partner = (ep, tp + 1 - 2 * core)
    above = (ep, tp + 2)
    below = (ep, tp - 2)
    has_low = z > 0
    has_high = z < Z - 1

    def column(d):
        index, bit = ep, 1
        while bit < E:
            if d & bit:
                index = index + bit * (1 - 2 * ((ep // bit) % 2))
            bit *= 2
        return (index, tp)

    local = [
        pltpu.make_async_copy(src, dst.at[0], lw_sem.at[i])
        for i, (src, dst) in enumerate(((gate, wg), (up, wu), (down, wd), (mixer, wm)))
    ]
    for copy in local:
        copy.start()
    barrier = pltpu.get_barrier_semaphore()
    for d in range(1, E):
        pl.semaphore_signal(barrier, inc=1, device_id=column(d), device_id_type=MESH)
    pl.semaphore_signal(barrier, inc=1, device_id=partner, device_id_type=MESH)

    @pl.when(has_low)
    def _():
        pl.semaphore_signal(barrier, inc=1, device_id=below, device_id_type=MESH)

    @pl.when(has_high)
    def _():
        pl.semaphore_signal(barrier, inc=1, device_id=above, device_id_type=MESH)

    x = tokens[...].astype(F32)
    x = x * lax.rsqrt(jnp.mean(x * x, axis=1, keepdims=True) + EPS) * expert_gain[...]
    normed[...] = x.astype(BF16)
    route = routes[...].astype(F32)
    s0, s1 = scores[:, 0:1], scores[:, 1:2]
    w0 = 1.0 / (1.0 + jnp.exp(s1 - s0))
    w1 = 1.0 / (1.0 + jnp.exp(s0 - s1))
    pieces = [route[:, 0:1], route[:, 1:2]]
    for p0, p1 in zip(split3(w0), split3(w1)):
        pieces += [p0.astype(F32), p1.astype(F32)]
    lane = lax.broadcasted_iota(jnp.int32, (C, TAGS), 1)
    tags = jnp.zeros((C, TAGS), F32)
    for i, piece in enumerate(pieces):
        tags = jnp.where(lane == i, piece, tags)
    xb[z, :, :B] = normed[:, A:]
    xb[z, :, B:] = tags.astype(BF16)

    pl.semaphore_wait(barrier, E + has_low.astype(jnp.int32) + has_high.astype(jnp.int32))

    def fwd_b(l, j, sems, dev):
        s = pl.ds(j * TB, TB)
        return rcopy(xb.at[l, s], xb.at[l, s], sems.at[l, j], fb_recv.at[l, j], dev)

    def fwd_a(l, j, sems, dev):
        s = pl.ds(j * R, R)
        return rcopy(xa.at[l, s], xa.at[l, s], sems.at[l, j], fa_recv.at[l, j], dev)

    def both_ways(make, chunks, up_sems, dn_sems):
        for j in range(chunks):

            @pl.when(has_high)
            def _():
                make(z, j, up_sems, above).start()

            @pl.when(has_low)
            def _():
                make(z, j, dn_sems, below).start()

    both_ways(fwd_b, B_CHUNKS, fb_up, fb_dn)

    row = lax.broadcasted_iota(jnp.int32, (C, C), 0)
    col = lax.broadcasted_iota(jnp.int32, (C, C), 1)
    before = (col < row).astype(F32).astype(BF16)
    later = (row > col).astype(F32).astype(BF16)
    slot = lax.broadcasted_iota(jnp.int32, (C, slots), 1)
    shift = cap.bit_length() - 1
    slot_expert = jnp.bitwise_xor(lax.shift_right_logical(slot, shift), ep).astype(F32)
    slot_rank = jnp.bitwise_and(slot, cap - 1).astype(F32)

    def selection(l, t):
        m0 = t[:, 0:1] == slot_expert
        m1 = t[:, 1:2] == slot_expert
        member = jnp.where(jnp.logical_or(m0, m1), 1.0, 0.0)
        rank = dot(before, member.astype(BF16))
        chosen = jnp.where(rank == slot_rank, member, 0.0)
        v0 = t[:, 2:3] + t[:, 4:5] + t[:, 6:7]
        v1 = t[:, 3:4] + t[:, 5:6] + t[:, 7:8]
        weight = chosen * jnp.where(m0, v0, v1)
        high = weight.astype(BF16)
        wh[l] = high
        wl[l] = (weight - high.astype(F32)).astype(BF16)
        return chosen.T.astype(BF16)

    def plane(src, dst, send, recv, d):
        s = pl.ds(d * cap, cap)
        return rcopy(src.at[s], dst.at[s], send, recv, column(d))

    def rest(src, dst, send, recv):
        s = pl.ds(cap, slots - cap)
        return rcopy(src.at[s], dst.at[s], send, recv, column(1))

    def dispatch_b(l, chosen):
        out = dot(chosen, xb[l, :, :B]).astype(BF16)
        xbs[l, :cap] = out[:cap]
        ob[l, cap:] = out[cap:]
        for d in range(1, E):
            plane(ob.at[l], xbs.at[l], pb_send.at[l], pb_recv.at[l], d).start()

    chosen = selection(z, tags)
    out = dot(chosen, normed[:, :A]).astype(BF16)
    xa[z, :cap] = out[:cap]
    oa[cap:] = out[cap:]
    for d in range(1, E):
        plane(oa, xa.at[z], pa_send, pa_recv, d).start()

    swaps = [
        rcopy(src, dst.at[1], pw_send.at[i], pw_recv.at[i], partner)
        for i, (src, dst) in enumerate(((gate, wg), (up, wu), (down, wd), (mixer, wm)))
    ]
    for swap in swaps:
        swap.start()

    heads = key.shape[1] // HEAD_DIM
    aw = key.shape[1]
    kv[:C, :aw] = jnp.concatenate(norm_heads(key, key_gain[...]), axis=1)
    kv[:C, aw:] = value[...]

    def kv_copy(d):
        return rcopy(kv.at[pl.ds(0, C)], kv.at[pl.ds(d * C, C)], kv_send.at[d], kv_recv.at[d], column(d))

    for d in range(1, E):
        kv_copy(d).start()

    dispatch_b(z, chosen)

    rest(oa, xa.at[z], pa_send, pa_recv).wait_recv()
    both_ways(fwd_a, A_CHUNKS, fa_up, fa_dn)

    def attention():
        for d in range(1, E):
            kv_copy(d).wait_recv()
        length = E * C
        query_norm = norm_heads(query, query_gain[...])
        lane = lax.broadcasted_iota(jnp.int32, (C, length), 1)
        bits = C.bit_length() - 1
        owner = jnp.bitwise_xor(lax.shift_right_logical(lane, bits), ep)
        key_place = owner * C + jnp.bitwise_and(lane, C - 1)
        query_place = ep * C + lax.broadcasted_iota(jnp.int32, (C, length), 0)
        allowed = key_place < query_place
        mixed = []
        for h in range(heads):
            part = slice(h * HEAD_DIM, (h + 1) * HEAD_DIM)
            vpart = slice(aw + h * HEAD_DIM, aw + (h + 1) * HEAD_DIM)
            s = dot_t(query_norm[h], kv[:, part]) * HEAD_DIM ** (-0.5) + offset[h]
            soft = jnp.log1p(jnp.exp(-jnp.abs(s)))
            rise = jnp.minimum(s, 0.0) - soft
            fail = jnp.where(allowed, jnp.minimum(-s, 0.0) - soft, 0.0)
            high, mid, low = split3(fail)
            sums = [
                jnp.sum(fail[:, d * C : (d + 1) * C], axis=1, keepdims=True) for d in range(E)
            ]
            afters = []
            for d in range(E):
                b = slice(d * C, (d + 1) * C)
                after = dot(high[:, b], later) + dot(mid[:, b], later) + dot(low[:, b], later)
                for o in range(E):
                    if o != d:
                        later_block = (column(o)[0] > column(d)[0]).astype(F32)
                        after = after + sums[o] * later_block
                afters.append(after)
            exponent = rise + jnp.concatenate(afters, axis=1)
            weights = jnp.where(allowed, jnp.exp(exponent), 0.0).astype(BF16)
            mixed.append(dot(weights, kv[:, vpart]))
        mixed = jnp.concatenate(mixed, axis=1).astype(BF16).astype(F32)
        rows = C // (2 * Z)
        for i in range(Z):
            for k in range(2):
                hm[i, k] = mixed[(2 * i + k) * rows : (2 * i + k + 1) * rows]

    hm_copy = rcopy(hm.at[:, 1 - core], hmo, hm_sem.at[0], hm_sem.at[1], partner)

    def mixer_terms():
        local[3].wait()
        swaps[3].wait_recv()
        hm_copy.wait_recv()
        rows = C // (2 * Z)
        mine = jnp.concatenate([hm[i, core] for i in range(Z)], axis=0).astype(BF16)
        other = jnp.concatenate([hmo[i] for i in range(Z)], axis=0).astype(BF16)
        terms = dot(mine, wm[0]) + dot(other, wm[1])
        for i in range(Z):
            ms[i] = terms[i * rows : (i + 1) * rows].astype(BF16)

    def expert(l):
        rest(ob.at[l], xbs.at[l], pb_send.at[l], pb_recv.at[l]).wait_recv()
        hidden = []
        for i in range(2):
            g = dot(xa[l], wg[i, :A]) + dot(xbs[l], wg[i, A:])
            u = dot(xa[l], wu[i, :A]) + dot(xbs[l], wu[i, A:])
            hidden.append((g / (1.0 + jnp.exp(-g)) * u).astype(BF16))
        tile = 256
        for start in range(A, wide, tile):
            c = slice(start, start + tile)
            y = (dot(hidden[0], wd[0, :, c]) + dot(hidden[1], wd[1, :, c])).astype(BF16)
            pb[l, :, start - A : start - A + tile] = y
        for d in range(1, E):
            plane(pb.at[l], qb.at[l], rb_send.at[l], rb_recv.at[l], d).start()
        qb[l, :cap] = pb[l, :cap]
        for start in range(0, A, tile):
            c = slice(start, start + tile)
            y = (dot(hidden[0], wd[0, :, c]) + dot(hidden[1], wd[1, :, c])).astype(BF16)
            pa[l, :, c] = y

    def ret_a(l, j, buf, recv, dev):
        s = pl.ds(j * R, R)
        return rcopy(pa.at[l, s], buf.at[l, s], za_send.at[l, j], recv.at[l, j], dev)

    def ret_b(l, j, buf, recv, dev):
        s = pl.ds(j * TB, TB)
        return rcopy(mb.at[l, s], buf.at[l, s], zb_send.at[l, j], recv.at[l, j], dev)

    def ret_m(l, buf, recv, dev):
        return rcopy(ms.at[l], buf.at[l], zm_send.at[l], recv.at[l], dev)

    def mix(l, s):
        return dot(wh[l, s], qb[l]) + dot(wl[l, s], qb[l])

    def returns(l, incoming, bufs, recvs, dev):
        for j in range(A_CHUNKS):
            s = pl.ds(j * R, R)

            @pl.when(incoming)
            def _():
                ret_a(l, j, bufs[0], recvs[0], dev).wait_recv()
                pa[l, s] = (pa[l, s].astype(F32) + bufs[0][l, s].astype(F32)).astype(BF16)

            ret_a(l, j, bufs[0], recvs[0], dev).start()

        @pl.when(incoming)
        def _():
            ret_m(l, bufs[2], recvs[2], dev).wait_recv()
            ms[l] = (ms[l].astype(F32) + bufs[2][l].astype(F32)).astype(BF16)

        ret_m(l, bufs[2], recvs[2], dev).start()
        rest(pb.at[l], qb.at[l], rb_send.at[l], rb_recv.at[l]).wait_recv()
        for j in range(B_CHUNKS):
            s = pl.ds(j * TB, TB)
            acc[...] = mix(l, s)

            @pl.when(incoming)
            def _():
                ret_b(l, j, bufs[1], recvs[1], dev).wait_recv()
                acc[...] = acc[...] + bufs[1][l, s].astype(F32)

            mb[l, s] = acc[...].astype(BF16)
            ret_b(l, j, bufs[1], recvs[1], dev).start()

    low_bufs, low_recvs = (ral, rbl, rml), (za_low, zb_low, zm_low)
    high_bufs, high_recvs = (rah, rbh, rmh), (za_high, zb_high, zm_high)

    def slot_step(t, carry):
        low_level, high_level = z - t, z + t
        low_live = low_level >= 0
        high_live = jnp.logical_and(high_level < Z, t > 0)

        @pl.when(t < Z)
        def _():
            @pl.when(t == 0)
            def _():
                attention()
                hm_copy.start()
                for copy in local[:3]:
                    copy.wait()
                for swap in swaps[:3]:
                    swap.wait_recv()

            @pl.when(t > 0)
            def _():
                def arrive(l, onward, sems, dev):
                    for j in range(B_CHUNKS):
                        fwd_b(l, j, sems, dev).wait_recv()

                        @pl.when(onward)
                        def _():
                            fwd_b(l, j, sems, dev).start()

                    dispatch_b(l, selection(l, xb[l, :, B:].astype(F32)))

                def arrive_a(l, onward, sems, dev):
                    for j in range(A_CHUNKS):
                        fwd_a(l, j, sems, dev).wait_recv()

                        @pl.when(onward)
                        def _():
                            fwd_a(l, j, sems, dev).start()

                @pl.when(low_live)
                def _():
                    arrive(low_level, has_high, fb_up, above)

                @pl.when(high_live)
                def _():
                    arrive(high_level, has_low, fb_dn, below)

                @pl.when(low_live)
                def _():
                    arrive_a(low_level, has_high, fa_up, above)

                @pl.when(high_live)
                def _():
                    arrive_a(high_level, has_low, fa_dn, below)

            def side(i, carry):
                expert(z + (2 * i - 1) * t)
                return carry

            lax.fori_loop(
                1 - low_live.astype(jnp.int32), 1 + high_live.astype(jnp.int32), side, 0
            )

            @pl.when(t == 0)
            def _():
                mixer_terms()

        target = t - z

        @pl.when(jnp.logical_and(target > z, target < Z))
        def _():
            returns(target, has_low, low_bufs, low_recvs, above)

        other = 2 * (Z - 1) - t - z

        @pl.when(jnp.logical_and(other >= 0, other < z))
        def _():
            returns(other, has_high, high_bufs, high_recvs, below)

        return carry

    lax.fori_loop(0, 2 * Z - 1, slot_step, 0)

    for j in range(A_CHUNKS):
        s = pl.ds(j * R, R)

        @pl.when(has_low)
        def _():
            ret_a(z, j, ral, za_low, above).wait_recv()
            pa[z, s] = (pa[z, s].astype(F32) + ral[z, s].astype(F32)).astype(BF16)

        @pl.when(has_high)
        def _():
            ret_a(z, j, rah, za_high, below).wait_recv()
            pa[z, s] = (pa[z, s].astype(F32) + rah[z, s].astype(F32)).astype(BF16)

        fa[s] = pa[z, s]
        if j == 0:
            qa[:cap] = pa[z, :cap]
        for d in range(max(1, j * R // cap), (j + 1) * R // cap):
            plane(fa, qa, ra_send, ra_recv, d).start()

    total = ms[z].astype(F32)
    att_out[...] = total.astype(BF16)

    @pl.when(has_low)
    def _():
        ret_m(z, rml, zm_low, above).wait_recv()
        att_out[...] = (att_out[...].astype(F32) + rml[z].astype(F32)).astype(BF16)

    @pl.when(has_high)
    def _():
        ret_m(z, rmh, zm_high, below).wait_recv()
        att_out[...] = (att_out[...].astype(F32) + rmh[z].astype(F32)).astype(BF16)

    rest(pb.at[z], qb.at[z], rb_send.at[z], rb_recv.at[z]).wait_recv()
    for j in range(B_CHUNKS):
        s = pl.ds(j * TB, TB)
        acc[...] = mix(z, s)

        @pl.when(has_low)
        def _():
            ret_b(z, j, rbl, zb_low, above).wait_recv()
            acc[...] = acc[...] + rbl[z, s].astype(F32)

        @pl.when(has_high)
        def _():
            ret_b(z, j, rbh, zb_high, below).wait_recv()
            acc[...] = acc[...] + rbh[z, s].astype(F32)

        exp_out[s, A:] = acc[...].astype(BF16)

    rest(fa, qa, ra_send, ra_recv).wait_recv()
    exp_out[:, :A] = (dot(wh[z], qa[...]) + dot(wl[z], qa[...])).astype(BF16)

    rest(oa, xa.at[z], pa_send, pa_recv).wait_send()
    rest(fa, qa, ra_send, ra_recv).wait_send()
    hm_copy.wait_send()
    for swap in swaps:
        swap.wait_send()
    for d in range(1, E):
        kv_copy(d).wait_send()

    def drain(l, carry):
        rest(ob.at[l], xbs.at[l], pb_send.at[l], pb_recv.at[l]).wait_send()
        rest(pb.at[l], qb.at[l], rb_send.at[l], rb_recv.at[l]).wait_send()

        @pl.when(jnp.logical_and(l <= z, has_high))
        def _():
            for j in range(B_CHUNKS):
                fwd_b(l, j, fb_up, above).wait_send()
            for j in range(A_CHUNKS):
                fwd_a(l, j, fa_up, above).wait_send()

        @pl.when(jnp.logical_and(l >= z, has_low))
        def _():
            for j in range(B_CHUNKS):
                fwd_b(l, j, fb_dn, below).wait_send()
            for j in range(A_CHUNKS):
                fwd_a(l, j, fa_dn, below).wait_send()

        @pl.when(l != z)
        def _():
            for j in range(A_CHUNKS):
                ret_a(l, j, ral, za_low, above).wait_send()
            for j in range(B_CHUNKS):
                ret_b(l, j, rbl, zb_low, above).wait_send()
            ret_m(l, rml, zm_low, above).wait_send()

        return carry

    lax.fori_loop(0, Z, drain, 0)


def layer(
    query, key, value, query_gain, key_gain, offset, mixer, tokens, expert_gain, routes, scores,
    gate, up, down,
):
    E = lax.axis_size("ep")
    Z = lax.axis_size("tp") // 2
    C, D = tokens.shape
    H = gate.shape[2]
    aw = key.shape[1]
    A = D * EARLY_SHARE // 256
    A -= A % 256
    B = D - A
    slots = TOP_K * C
    rows = C // (2 * Z)
    dma = lambda *shape: pltpu.SemaphoreType.DMA(shape)
    vmem = pl.BlockSpec(memory_space=pltpu.VMEM)
    smem = pl.BlockSpec(memory_space=pltpu.SMEM)
    hbm = pl.BlockSpec(memory_space=pl.ANY)
    kernel = functools.partial(body, E, Z, C, D, A)
    NA, NB = A_CHUNKS, B_CHUNKS
    return pl.pallas_call(
        kernel,
        name="step",
        out_shape=(
            jax.ShapeDtypeStruct((rows, D), BF16),
            jax.ShapeDtypeStruct((C, D), BF16),
        ),
        in_specs=[vmem, vmem, vmem, vmem, vmem, smem, hbm, vmem, vmem, vmem, vmem, hbm, hbm, hbm],
        out_specs=(vmem, vmem),
        scratch_shapes=[
            pltpu.VMEM((2, D, H), BF16),
            pltpu.VMEM((2, D, H), BF16),
            pltpu.VMEM((2, H, D), BF16),
            pltpu.VMEM((2, aw, D), BF16),
            pltpu.VMEM((C, D), BF16),
            pltpu.VMEM((Z, C, B + TAGS), BF16),
            pltpu.VMEM((Z, slots, A), BF16),
            pltpu.VMEM((Z, slots, B), BF16),
            pltpu.VMEM((slots, A), BF16),
            pltpu.VMEM((Z, slots, B), BF16),
            pltpu.VMEM((Z, slots, A), BF16),
            pltpu.VMEM((Z, slots, B), BF16),
            pltpu.VMEM((Z, slots, B), BF16),
            pltpu.VMEM((slots, A), BF16),
            pltpu.VMEM((Z, C, slots), BF16),
            pltpu.VMEM((Z, C, slots), BF16),
            pltpu.VMEM((Z, slots, A), BF16),
            pltpu.VMEM((Z, slots, A), BF16),
            pltpu.VMEM((Z, C, B), BF16),
            pltpu.VMEM((Z, C, B), BF16),
            pltpu.VMEM((Z, C, B), BF16),
            pltpu.VMEM((slots, A), BF16),
            pltpu.VMEM((C // NB, B), F32),
            pltpu.VMEM((E * C, 2 * aw), BF16),
            pltpu.VMEM((Z, 2, rows, aw), F32),
            pltpu.VMEM((Z, rows, aw), F32),
            pltpu.VMEM((Z, rows, D), BF16),
            pltpu.VMEM((Z, rows, D), BF16),
            pltpu.VMEM((Z, rows, D), BF16),
            dma(4), dma(4), dma(4), dma(2),
            pltpu.SemaphoreType.DMA, pltpu.SemaphoreType.DMA,
            dma(E), dma(E),
            dma(Z), dma(Z),
            dma(Z), dma(Z),
            pltpu.SemaphoreType.DMA, pltpu.SemaphoreType.DMA,
            dma(Z, NB), dma(Z, NB), dma(Z, NB),
            dma(Z, NA), dma(Z, NA), dma(Z, NA),
            dma(Z, NA), dma(Z, NA), dma(Z, NA),
            dma(Z, NB), dma(Z, NB), dma(Z, NB),
            dma(Z), dma(Z), dma(Z),
        ],
        compiler_params=pltpu.CompilerParams(
            collective_id=0, has_side_effects=True, vmem_limit_bytes=62 * 1024 * 1024
        ),
    )(
        query, key, value, query_gain[None], key_gain[None], offset, mixer, tokens,
        expert_gain[None], routes, scores, gate[0], up[0], down[0],
    )


def solution(mesh):
    in_specs = (
        P("ep", "tp"),
        P("ep", "tp"),
        P("ep", "tp"),
        P(),
        P(),
        P("tp"),
        P("tp", None),
        P(("ep", "tp"), None),
        P(),
        P(("ep", "tp"), None),
        P(("ep", "tp"), None),
        P("ep", None, "tp"),
        P("ep", None, "tp"),
        P("ep", "tp", None),
    )
    out_specs = (P(("ep", "tp"), None), P(("ep", "tp"), None))
    return jax.shard_map(layer, mesh=mesh, in_specs=in_specs, out_specs=out_specs, check_vma=False)
```

profile of v0, /device:TPU:0, one launch (start us, length us, event | category | flops | bytes accessed | tf_op | source)
XLA Modules:
  0.0 131.6 jit_solution(17853140751196974144)
XLA Ops:
  0.6 1.4 %copy.18.routes = s32[128,2]{1,0:T(8,128)} copy(s32[128,2]{0,1:T(2,128)} %param.23) | data formatting | bytes 2048 | tf_op args[9]
  2.0 1.4 %copy.19.scores = f32[128,2]{1,0:T(8,128)} copy(f32[128,2]{0,1:T(2,128)} %param.24) | data formatting | bytes 2048 | tf_op args[10]
  3.5 0.0 copy-start
  3.5 4.0 %copy.16 = bf16[1,2048,448]{2,1,0:T(8,128)(2,1)} copy(bf16[1,2048,448]{1,2,0:T(8,128)(2,1)} %param.25) | data formatting | bytes 3670016 | tf_op args[11]
  7.4 0.0 copy-done
  7.4 2.4 %copy.17 = bf16[1,2048,448]{2,1,0:T(8,128)(2,1)} copy(bf16[1,2048,448]{1,2,0:T(8,128)(2,1)S(1)} %copy-done) | data formatting | bytes 3670016 | tf_op args[12]
  9.9 118.3 %step.1 = (bf16[16,2048]{1,0:T(8,128)(2,1)}, bf16[128,2048]{1,0:T(8,128)(2,1)}) custom-call(bf16[128,256]{1,0:T(8,128)(2,1)} %query.1, bf16[128,256]{1,0:T(8,128)(2,1)} %key.1, bf16[128,256]{1,0:T(8,128)(2,1)} %value.1, f32[1,64]{1,0:T(1,128)} %bitcast.10, f32[1,64]{1,0:T(1,128)} %bitcast.11, f32[4]{0:T(128)} %offset.1, bf16[256,2048]{1,0:T(8,128)(2,1)} %mixer.1, ...), custom_call_target="tpu_custom_call" | custom-call | tf_op jit(solution)/shard_map/step/pallas_call | solution.py:528
  128.2 1.5 %copy.22 = bf16[16,2048]{1,0:T(8,128)(2,1)} copy(bf16[16,2048]{1,0:T(8,128)(2,1)} %get-tuple-element.4) | data formatting | bytes 131072
  129.7 1.9 %copy.23 = bf16[128,2048]{1,0:T(8,128)(2,1)} copy(bf16[128,2048]{1,0:T(8,128)(2,1)} %get-tuple-element.5) | data formatting | bytes 1048576
Async XLA Ops:
  3.5 4.0 %copy-start = (bf16[1,2048,448]{1,2,0:T(8,128)(2,1)S(1)}, bf16[1,2048,448]{1,2,0:T(8,128)(2,1)}, u32[]{:S(2)}) copy-start(bf16[1,2048,448]{1,2,0:T(8,128)(2,1)} %param.26) | copy-start | bytes 5505028
where the time goes:
time: 132 us
  Pallas kernels  118 us (89%)
  local copies, waits for them, and re-layouts  12.6 us (10%)
    pallas_call x1, Pallas kernels, layer(): pl.pallas_call(kernel, name='step', out_shape=(jax.ShapeDtypeStruct((rows...  118 us
    unnamed x8, local copies, waits for them, and re-layouts  12.6 us

commit v1 on v0

--- a/solution.py
+++ b/solution.py
@@ -17,6 +17,7 @@
 EARLY_SHARE = 96
 A_CHUNKS = 4
 B_CHUNKS = 2
+B_BACK = 4
 
 
 def dot(a, b):
@@ -68,6 +69,7 @@
     cap = slots // E
     R = slots // A_CHUNKS
     TB = C // B_CHUNKS
+    TR = C // B_BACK
     ep = lax.axis_index("ep")
     tp = lax.axis_index("tp")
     z = tp // 2
@@ -109,20 +111,19 @@
     x = x * lax.rsqrt(jnp.mean(x * x, axis=1, keepdims=True) + EPS) * expert_gain[...]
     normed[...] = x.astype(BF16)
     route = routes[...].astype(F32)
-    s0, s1 = scores[:, 0:1], scores[:, 1:2]
+    s0, s1 = scores[0:1], scores[1:2]
     w0 = 1.0 / (1.0 + jnp.exp(s1 - s0))
     w1 = 1.0 / (1.0 + jnp.exp(s0 - s1))
-    pieces = [route[:, 0:1], route[:, 1:2]]
+    pieces = [route[0:1], route[1:2]]
     for p0, p1 in zip(split3(w0), split3(w1)):
         pieces += [p0.astype(F32), p1.astype(F32)]
-    lane = lax.broadcasted_iota(jnp.int32, (C, TAGS), 1)
-    tags = jnp.zeros((C, TAGS), F32)
+    line = lax.broadcasted_iota(jnp.int32, (TAGS, C), 0)
+    tags = jnp.zeros((TAGS, C), F32)
     for i, piece in enumerate(pieces):
-        tags = jnp.where(lane == i, piece, tags)
+        tags = jnp.where(line == i, piece, tags)
+    tags = tags.T
     xb[z, :, :B] = normed[:, A:]
     xb[z, :, B:] = tags.astype(BF16)
-
-    pl.semaphore_wait(barrier, E + has_low.astype(jnp.int32) + has_high.astype(jnp.int32))
 
     def fwd_b(l, j, sems, dev):
         s = pl.ds(j * TB, TB)
@@ -142,8 +143,6 @@
             @pl.when(has_low)
             def _():
                 make(z, j, dn_sems, below).start()
-
-    both_ways(fwd_b, B_CHUNKS, fb_up, fb_dn)
 
     row = lax.broadcasted_iota(jnp.int32, (C, C), 0)
     col = lax.broadcasted_iota(jnp.int32, (C, C), 1)
@@ -187,6 +186,10 @@
     out = dot(chosen, normed[:, :A]).astype(BF16)
     xa[z, :cap] = out[:cap]
     oa[cap:] = out[cap:]
+    with jax.named_scope("barrier"):
+     pl.semaphore_wait(barrier, E + has_low.astype(jnp.int32) + has_high.astype(jnp.int32))
+
+    both_ways(fwd_b, B_CHUNKS, fb_up, fb_dn)
     for d in range(1, E):
         plane(oa, xa.at[z], pa_send, pa_recv, d).start()
 
@@ -197,6 +200,46 @@
     for swap in swaps:
         swap.start()
 
+    dispatch_b(z, chosen)
+
+    with jax.named_scope("w_own_a"):
+        rest(oa, xa.at[z], pa_send, pa_recv).wait_recv()
+    both_ways(fwd_a, A_CHUNKS, fa_up, fa_dn)
+
+    def on_sides(t, work):
+        @pl.when(z - t >= 0)
+        def _():
+            work(z - t, has_high, 0)
+
+        @pl.when(z + t < Z)
+        def _():
+            work(z + t, has_low, 1)
+
+    def arrive_b(l, onward, side):
+        sems, dev = ((fb_up, above), (fb_dn, below))[side]
+        for j in range(B_CHUNKS):
+            with jax.named_scope("w_fwd_b"):
+                fwd_b(l, j, sems, dev).wait_recv()
+
+            @pl.when(onward)
+            def _():
+                fwd_b(l, j, sems, dev).start()
+
+        with jax.named_scope("dispatch"):
+            dispatch_b(l, selection(l, xb[l, :, B:].astype(F32)))
+
+    def arrive_a(l, onward, side):
+        sems, dev = ((fa_up, above), (fa_dn, below))[side]
+        for j in range(A_CHUNKS):
+            with jax.named_scope("w_fwd_a"):
+                fwd_a(l, j, sems, dev).wait_recv()
+
+            @pl.when(onward)
+            def _():
+                fwd_a(l, j, sems, dev).start()
+
+    on_sides(1, arrive_b)
+
     heads = key.shape[1] // HEAD_DIM
     aw = key.shape[1]
     kv[:C, :aw] = jnp.concatenate(norm_heads(key, key_gain[...]), axis=1)
@@ -208,13 +251,9 @@
     for d in range(1, E):
         kv_copy(d).start()
 
-    dispatch_b(z, chosen)
-
-    rest(oa, xa.at[z], pa_send, pa_recv).wait_recv()
-    both_ways(fwd_a, A_CHUNKS, fa_up, fa_dn)
-
     def attention():
-        for d in range(1, E):
+        with jax.named_scope("w_kv"):
+         for d in range(1, E):
             kv_copy(d).wait_recv()
         length = E * C
         query_norm = norm_heads(query, query_gain[...])
@@ -257,9 +296,10 @@
     hm_copy = rcopy(hm.at[:, 1 - core], hmo, hm_sem.at[0], hm_sem.at[1], partner)
 
     def mixer_terms():
-        local[3].wait()
-        swaps[3].wait_recv()
-        hm_copy.wait_recv()
+        with jax.named_scope("w_mixer"):
+         local[3].wait()
+         swaps[3].wait_recv()
+         hm_copy.wait_recv()
         rows = C // (2 * Z)
         mine = jnp.concatenate([hm[i, core] for i in range(Z)], axis=0).astype(BF16)
         other = jnp.concatenate([hmo[i] for i in range(Z)], axis=0).astype(BF16)
@@ -268,31 +308,34 @@
             ms[i] = terms[i * rows : (i + 1) * rows].astype(BF16)
 
     def expert(l):
-        rest(ob.at[l], xbs.at[l], pb_send.at[l], pb_recv.at[l]).wait_recv()
+        with jax.named_scope("w_plane_b"):
+         rest(ob.at[l], xbs.at[l], pb_send.at[l], pb_recv.at[l]).wait_recv()
         hidden = []
         for i in range(2):
-            g = dot(xa[l], wg[i, :A]) + dot(xbs[l], wg[i, A:])
-            u = dot(xa[l], wu[i, :A]) + dot(xbs[l], wu[i, A:])
+            g = dot_t(xa[l], wg[i, :, :A]) + dot_t(xbs[l], wg[i, :, A:])
+            u = dot_t(xa[l], wu[i, :, :A]) + dot_t(xbs[l], wu[i, :, A:])
             hidden.append((g / (1.0 + jnp.exp(-g)) * u).astype(BF16))
-        tile = 256
+        tile = 128 if A % 256 else 256
         for start in range(A, wide, tile):
             c = slice(start, start + tile)
             y = (dot(hidden[0], wd[0, :, c]) + dot(hidden[1], wd[1, :, c])).astype(BF16)
             pb[l, :, start - A : start - A + tile] = y
-        for d in range(1, E):
-            plane(pb.at[l], qb.at[l], rb_send.at[l], rb_recv.at[l], d).start()
-        qb[l, :cap] = pb[l, :cap]
         for start in range(0, A, tile):
             c = slice(start, start + tile)
             y = (dot(hidden[0], wd[0, :, c]) + dot(hidden[1], wd[1, :, c])).astype(BF16)
             pa[l, :, c] = y
 
+    def send_home(l):
+        for d in range(1, E):
+            plane(pb.at[l], qb.at[l], rb_send.at[l], rb_recv.at[l], d).start()
+        qb[l, :cap] = pb[l, :cap]
+
     def ret_a(l, j, buf, recv, dev):
         s = pl.ds(j * R, R)
         return rcopy(pa.at[l, s], buf.at[l, s], za_send.at[l, j], recv.at[l, j], dev)
 
     def ret_b(l, j, buf, recv, dev):
-        s = pl.ds(j * TB, TB)
+        s = pl.ds(j * TR, TR)
         return rcopy(mb.at[l, s], buf.at[l, s], zb_send.at[l, j], recv.at[l, j], dev)
 
     def ret_m(l, buf, recv, dev):
@@ -301,130 +344,157 @@
     def mix(l, s):
         return dot(wh[l, s], qb[l]) + dot(wl[l, s], qb[l])
 
-    def returns(l, incoming, bufs, recvs, dev):
+    def returns_a(l, incoming, side):
+        buf, recv, dev = ((ral, za_low, above), (rah, za_high, below))[side]
         for j in range(A_CHUNKS):
             s = pl.ds(j * R, R)
 
             @pl.when(incoming)
             def _():
-                ret_a(l, j, bufs[0], recvs[0], dev).wait_recv()
-                pa[l, s] = (pa[l, s].astype(F32) + bufs[0][l, s].astype(F32)).astype(BF16)
-
-            ret_a(l, j, bufs[0], recvs[0], dev).start()
+                with jax.named_scope("w_ret_a"):
+                    ret_a(l, j, buf, recv, dev).wait_recv()
+                pa[l, s] = (pa[l, s].astype(F32) + buf[l, s].astype(F32)).astype(BF16)
+
+            ret_a(l, j, buf, recv, dev).start()
+
+    def returns_m(l, incoming, side):
+        buf, recv, dev = ((rml, zm_low, above), (rmh, zm_high, below))[side]
 
         @pl.when(incoming)
         def _():
-            ret_m(l, bufs[2], recvs[2], dev).wait_recv()
-            ms[l] = (ms[l].astype(F32) + bufs[2][l].astype(F32)).astype(BF16)
-
-        ret_m(l, bufs[2], recvs[2], dev).start()
-        rest(pb.at[l], qb.at[l], rb_send.at[l], rb_recv.at[l]).wait_recv()
-        for j in range(B_CHUNKS):
-            s = pl.ds(j * TB, TB)
+            ret_m(l, buf, recv, dev).wait_recv()
+            ms[l] = (ms[l].astype(F32) + buf[l].astype(F32)).astype(BF16)
+
+        ret_m(l, buf, recv, dev).start()
+
+    def returns_b(l, incoming, side):
+        buf, recv, dev = ((rbl, zb_low, above), (rbh, zb_high, below))[side]
+        with jax.named_scope("w_ret_plane"):
+            rest(pb.at[l], qb.at[l], rb_send.at[l], rb_recv.at[l]).wait_recv()
+        for j in range(B_BACK):
+            s = pl.ds(j * TR, TR)
             acc[...] = mix(l, s)
 
             @pl.when(incoming)
             def _():
-                ret_b(l, j, bufs[1], recvs[1], dev).wait_recv()
-                acc[...] = acc[...] + bufs[1][l, s].astype(F32)
+                with jax.named_scope("w_ret_b"):
+                    ret_b(l, j, buf, recv, dev).wait_recv()
+                acc[...] = acc[...] + buf[l, s].astype(F32)
 
             mb[l, s] = acc[...].astype(BF16)
-            ret_b(l, j, bufs[1], recvs[1], dev).start()
-
-    low_bufs, low_recvs = (ral, rbl, rml), (za_low, zb_low, zm_low)
-    high_bufs, high_recvs = (rah, rbh, rmh), (za_high, zb_high, zm_high)
+            ret_b(l, j, buf, recv, dev).start()
+
+    def on_targets(t, work):
+        target = t - z
+
+        @pl.when(jnp.logical_and(target > z, target < Z))
+        def _():
+            work(target, has_low, 0)
+
+        other = 2 * (Z - 1) - t - z
+
+        @pl.when(jnp.logical_and(other >= 0, other < z))
+        def _():
+            work(other, has_high, 1)
+
+    def levels_of(t, work):
+        low = (z - t >= 0).astype(jnp.int32)
+        high = jnp.logical_and(z + t < Z, t > 0).astype(jnp.int32)
+
+        def side(i, carry):
+            work(z + (2 * i - 1) * t)
+            return carry
+
+        lax.fori_loop(1 - low, 1 + high, side, 0)
+
+    with jax.named_scope("w_weights"):
+        for copy in local[:3]:
+            copy.wait()
+        for swap in swaps[:3]:
+            swap.wait_recv()
+
+    def tail_m(t, carry):
+        on_targets(t, returns_m)
+        return carry
+
+    at_end = jnp.logical_or(z == 0, z == Z - 1)
 
     def slot_step(t, carry):
-        low_level, high_level = z - t, z + t
-        low_live = low_level >= 0
-        high_live = jnp.logical_and(high_level < Z, t > 0)
-
-        @pl.when(t < Z)
-        def _():
-            @pl.when(t == 0)
+        with jax.named_scope("expert"):
+            levels_of(t, expert)
+
+        with jax.named_scope("ret_a"):
+            on_targets(t, returns_a)
+
+        @pl.when(jnp.logical_and(t > 0, t < Z - 1))
+        def _():
+            on_sides(t + 1, arrive_b)
+
+        @pl.when(t > 0)
+        def _():
+            levels_of(t, send_home)
+
+        @pl.when(t == Z - 1)
+        def _():
+            send_home(z)
+
+        with jax.named_scope("ret_b"):
+            on_targets(t - 1, returns_b)
+
+        @pl.when(t == 1)
+        def _():
+            with jax.named_scope("attention"):
+                attention()
+            hm_copy.start()
+
+        @pl.when(t < Z - 1)
+        def _():
+            on_sides(t + 1, arrive_a)
+
+        @pl.when(t == 1)
+        def _():
+            with jax.named_scope("mixer"):
+                mixer_terms()
+
+            @pl.when(at_end)
             def _():
-                attention()
-                hm_copy.start()
-                for copy in local[:3]:
-                    copy.wait()
-                for swap in swaps[:3]:
-                    swap.wait_recv()
-
-            @pl.when(t > 0)
-            def _():
-                def arrive(l, onward, sems, dev):
-                    for j in range(B_CHUNKS):
-                        fwd_b(l, j, sems, dev).wait_recv()
-
-                        @pl.when(onward)
-                        def _():
-                            fwd_b(l, j, sems, dev).start()
-
-                    dispatch_b(l, selection(l, xb[l, :, B:].astype(F32)))
-
-                def arrive_a(l, onward, sems, dev):
-                    for j in range(A_CHUNKS):
-                        fwd_a(l, j, sems, dev).wait_recv()
-
-                        @pl.when(onward)
-                        def _():
-                            fwd_a(l, j, sems, dev).start()
-
-                @pl.when(low_live)
-                def _():
-                    arrive(low_level, has_high, fb_up, above)
-
-                @pl.when(high_live)
-                def _():
-                    arrive(high_level, has_low, fb_dn, below)
-
-                @pl.when(low_live)
-                def _():
-                    arrive_a(low_level, has_high, fa_up, above)
-
-                @pl.when(high_live)
-                def _():
-                    arrive_a(high_level, has_low, fa_dn, below)
-
-            def side(i, carry):
-                expert(z + (2 * i - 1) * t)
-                return carry
-
-            lax.fori_loop(
-                1 - low_live.astype(jnp.int32), 1 + high_live.astype(jnp.int32), side, 0
-            )
-
-            @pl.when(t == 0)
-            def _():
-                mixer_terms()
-
-        target = t - z
-
-        @pl.when(jnp.logical_and(target > z, target < Z))
-        def _():
-            returns(target, has_low, low_bufs, low_recvs, above)
-
-        other = 2 * (Z - 1) - t - z
-
-        @pl.when(jnp.logical_and(other >= 0, other < z))
-        def _():
-            returns(other, has_high, high_bufs, high_recvs, below)
+                lax.fori_loop(1, 2 * Z - 1, tail_m, 0)
 
         return carry
 
-    lax.fori_loop(0, 2 * Z - 1, slot_step, 0)
+    lax.fori_loop(0, Z, slot_step, 0)
+
+    @pl.when(jnp.logical_not(at_end))
+    def _():
+        with jax.named_scope("tail_m"):
+            lax.fori_loop(1, 2 * Z - 1, tail_m, 0)
+
+    def tail_a(t, carry):
+        with jax.named_scope("tail_a"):
+            on_targets(t, returns_a)
+        return carry
+
+    def tail_b(t, carry):
+        with jax.named_scope("tail_b"):
+            on_targets(t, returns_b)
+        return carry
+
+    lax.fori_loop(Z, 2 * Z - 1, tail_a, 0)
+    lax.fori_loop(Z - 1, 2 * Z - 1, tail_b, 0)
 
     for j in range(A_CHUNKS):
         s = pl.ds(j * R, R)
 
         @pl.when(has_low)
         def _():
-            ret_a(z, j, ral, za_low, above).wait_recv()
+            with jax.named_scope("f_a_low"):
+             ret_a(z, j, ral, za_low, above).wait_recv()
             pa[z, s] = (pa[z, s].astype(F32) + ral[z, s].astype(F32)).astype(BF16)
 
         @pl.when(has_high)
         def _():
-            ret_a(z, j, rah, za_high, below).wait_recv()
+            with jax.named_scope("f_a_high"):
+             ret_a(z, j, rah, za_high, below).wait_recv()
             pa[z, s] = (pa[z, s].astype(F32) + rah[z, s].astype(F32)).astype(BF16)
 
         fa[s] = pa[z, s]
@@ -438,7 +508,8 @@
 
     @pl.when(has_low)
     def _():
-        ret_m(z, rml, zm_low, above).wait_recv()
+        with jax.named_scope("f_m"):
+            ret_m(z, rml, zm_low, above).wait_recv()
         att_out[...] = (att_out[...].astype(F32) + rml[z].astype(F32)).astype(BF16)
 
     @pl.when(has_high)
@@ -447,23 +518,26 @@
         att_out[...] = (att_out[...].astype(F32) + rmh[z].astype(F32)).astype(BF16)
 
     rest(pb.at[z], qb.at[z], rb_send.at[z], rb_recv.at[z]).wait_recv()
-    for j in range(B_CHUNKS):
-        s = pl.ds(j * TB, TB)
+    for j in range(B_BACK):
+        s = pl.ds(j * TR, TR)
         acc[...] = mix(z, s)
 
         @pl.when(has_low)
         def _():
-            ret_b(z, j, rbl, zb_low, above).wait_recv()
+            with jax.named_scope("f_b_low"):
+             ret_b(z, j, rbl, zb_low, above).wait_recv()
             acc[...] = acc[...] + rbl[z, s].astype(F32)
 
         @pl.when(has_high)
         def _():
-            ret_b(z, j, rbh, zb_high, below).wait_recv()
+            with jax.named_scope("f_b_high"):
+             ret_b(z, j, rbh, zb_high, below).wait_recv()
             acc[...] = acc[...] + rbh[z, s].astype(F32)
 
         exp_out[s, A:] = acc[...].astype(BF16)
 
-    rest(fa, qa, ra_send, ra_recv).wait_recv()
+    with jax.named_scope("f_plane_a"):
+     rest(fa, qa, ra_send, ra_recv).wait_recv()
     exp_out[:, :A] = (dot(wh[z], qa[...]) + dot(wl[z], qa[...])).astype(BF16)
 
     rest(oa, xa.at[z], pa_send, pa_recv).wait_send()
@@ -496,7 +570,7 @@
         def _():
             for j in range(A_CHUNKS):
                 ret_a(l, j, ral, za_low, above).wait_send()
-            for j in range(B_CHUNKS):
+            for j in range(B_BACK):
                 ret_b(l, j, rbl, zb_low, above).wait_send()
             ret_m(l, rml, zm_low, above).wait_send()
 
@@ -515,7 +589,7 @@
     H = gate.shape[2]
     aw = key.shape[1]
     A = D * EARLY_SHARE // 256
-    A -= A % 256
+    A -= A % 128
     B = D - A
     slots = TOP_K * C
     rows = C // (2 * Z)
@@ -525,7 +599,7 @@
     hbm = pl.BlockSpec(memory_space=pl.ANY)
     kernel = functools.partial(body, E, Z, C, D, A)
     NA, NB = A_CHUNKS, B_CHUNKS
-    return pl.pallas_call(
+    results = pl.pallas_call(
         kernel,
         name="step",
         out_shape=(
@@ -535,8 +609,8 @@
         in_specs=[vmem, vmem, vmem, vmem, vmem, smem, hbm, vmem, vmem, vmem, vmem, hbm, hbm, hbm],
         out_specs=(vmem, vmem),
         scratch_shapes=[
-            pltpu.VMEM((2, D, H), BF16),
-            pltpu.VMEM((2, D, H), BF16),
+            pltpu.VMEM((2, H, D), BF16),
+            pltpu.VMEM((2, H, D), BF16),
             pltpu.VMEM((2, H, D), BF16),
             pltpu.VMEM((2, aw, D), BF16),
             pltpu.VMEM((C, D), BF16),
@@ -557,7 +631,7 @@
             pltpu.VMEM((Z, C, B), BF16),
             pltpu.VMEM((Z, C, B), BF16),
             pltpu.VMEM((slots, A), BF16),
-            pltpu.VMEM((C // NB, B), F32),
+            pltpu.VMEM((C // B_BACK, B), F32),
             pltpu.VMEM((E * C, 2 * aw), BF16),
             pltpu.VMEM((Z, 2, rows, aw), F32),
             pltpu.VMEM((Z, rows, aw), F32),
@@ -573,7 +647,7 @@
             dma(Z, NB), dma(Z, NB), dma(Z, NB),
             dma(Z, NA), dma(Z, NA), dma(Z, NA),
             dma(Z, NA), dma(Z, NA), dma(Z, NA),
-            dma(Z, NB), dma(Z, NB), dma(Z, NB),
+            dma(Z, B_BACK), dma(Z, B_BACK), dma(Z, B_BACK),
             dma(Z), dma(Z), dma(Z),
         ],
         compiler_params=pltpu.CompilerParams(
@@ -581,8 +655,28 @@
         ),
     )(
         query, key, value, query_gain[None], key_gain[None], offset, mixer, tokens,
-        expert_gain[None], routes, scores, gate[0], up[0], down[0],
+        expert_gain[None], routes.T, scores.T, gate[0].T, up[0].T, down[0],
     )
+    return pl.pallas_call(
+        hand_over,
+        name="hand_over",
+        out_shape=(
+            jax.ShapeDtypeStruct((rows, D), BF16),
+            jax.ShapeDtypeStruct((C, D), BF16),
+        ),
+        in_specs=[vmem, vmem],
+        out_specs=(hbm, hbm),
+        scratch_shapes=[dma(2)],
+    )(*results)
+
+
+def hand_over(att_in, exp_in, att_out, exp_out, sems):
+    first = pltpu.make_async_copy(att_in, att_out, sems.at[0])
+    second = pltpu.make_async_copy(exp_in, exp_out, sems.at[1])
+    second.start()
+    first.start()
+    second.wait()
+    first.wait()
 
 
 def solution(mesh):

time: 132 us -> 98.7 us (0.75)
  Pallas kernels: 118 us -> 97.9 us
  local copies, waits for them, and re-layouts: 12.6 us -> 0 us
    pallas_call x1, Pallas kernels: 118 us -> 96 us  [layer(): pl.pallas_call(kernel, name='step', out_shape=(jax.ShapeDtypeStruct((rows...]
    unnamed x8 -> x0, local copies, waits for them, and re-layouts: 12.6 us -> none
    pallas_call x0 -> x1, Pallas kernels: none -> 1.9 us  [layer(): pl.pallas_call(hand_over, name='hand_over', out_shape=(jax.ShapeDtypeStru...]
where the time goes in v1:
time: 98.7 us; the launch traced here: 98.5 us
  Pallas kernels  97.9 us (99%)
    pallas_call x1, Pallas kernels, layer(): pl.pallas_call(kernel, name='step', out_shape=(jax.ShapeDtypeStruct((rows...  96 us

profile of v1, /device:TPU:0, one launch (start us, length us, event | category | flops | bytes accessed | tf_op | source)
XLA Modules:
  0.0 98.5 jit_solution(11989428024851985620)
XLA Ops:
  0.6 96.0 %step.1 = (bf16[16,2048]{1,0:T(8,128)(2,1)}, bf16[128,2048]{1,0:T(8,128)(2,1)}) custom-call(bf16[128,256]{1,0:T(8,128)(2,1)} %query.1, bf16[128,256]{1,0:T(8,128)(2,1)} %key.1, bf16[128,256]{1,0:T(8,128)(2,1)} %value.1, f32[1,64]{1,0:T(1,128)} %bitcast.18, f32[1,64]{1,0:T(1,128)} %bitcast.19, f32[4]{0:T(128)} %offset.1, bf16[256,2048]{1,0:T(8,128)(2,1)} %mixer.1, ...), custom_call_target="tpu_custom_call" | custom-call | tf_op jit(solution)/shard_map/step/pallas_call | solution.py:602
  96.6 1.9 %hand_over.1 = (bf16[16,2048]{1,0:T(8,128)(2,1)}, bf16[128,2048]{1,0:T(8,128)(2,1)}) custom-call(bf16[16,2048]{1,0:T(8,128)(2,1)} %get-tuple-element.4.att_in, bf16[128,2048]{1,0:T(8,128)(2,1)} %get-tuple-element.5.exp_in), custom_call_target="tpu_custom_call" | custom-call | tf_op jit(solution)/shard_map/hand_over/pallas_call | solution.py:660

commit v2 on v1

--- a/solution.py
+++ b/solution.py
@@ -10,14 +10,15 @@
 HEAD_DIM = 64
 TOP_K = 2
 EPS = 1e-06
-TAGS = 128
+TAGS = 8
 MESH = pl.DeviceIdType.MESH
 F32, BF16 = jnp.float32, jnp.bfloat16
 
 EARLY_SHARE = 96
 A_CHUNKS = 4
+A_BACK = 4
 B_CHUNKS = 2
-B_BACK = 4
+B_BACK = 8
 
 
 def dot(a, b):
@@ -53,14 +54,15 @@
 
 def body(
     experts, levels, count, wide, early,
-    query, key, value, query_gain, key_gain, offset, mixer, tokens, expert_gain, routes, scores,
-    gate, up, down,
+    query_in, key_in, value_in, query_gain_in, key_gain_in, offset_in, mixer, tokens_in,
+    expert_gain_in, routes_in, scores_in, gate, up, down,
     att_out, exp_out,
-    wg, wu, wd, wm, normed, xb, xa, xbs, oa, ob, pa, pb, qb, qa, wh, wl,
+    query, key, value, query_gain, key_gain, offset, tokens, expert_gain, routes, scores, in_sem,
+    wg, wu, wd, wm, normed, tg, xb, xa, xbs, oa, ob, pa, pb, qb, qa, wh, wl,
     ral, rah, mb, rbl, rbh, fa, acc, kv, hm, hmo, ms, rml, rmh,
     lw_sem, pw_send, pw_recv, hm_sem,
     pa_send, pa_recv, kv_send, kv_recv, pb_send, pb_recv, rb_send, rb_recv, ra_send, ra_recv,
-    fb_up, fb_dn, fb_recv, fa_up, fa_dn, fa_recv,
+    ft_up, ft_dn, ft_recv, fb_up, fb_dn, fb_recv, fa_up, fa_dn, fa_recv,
     za_send, za_low, za_high, zb_send, zb_low, zb_high, zm_send, zm_low, zm_high,
 ):
     E, Z, C = experts, levels, count
@@ -70,6 +72,7 @@
     R = slots // A_CHUNKS
     TB = C // B_CHUNKS
     TR = C // B_BACK
+    RR = slots // A_BACK
     ep = lax.axis_index("ep")
     tp = lax.axis_index("tp")
     z = tp // 2
@@ -88,24 +91,35 @@
             bit *= 2
         return (index, tp)
 
+    barrier = pltpu.get_barrier_semaphore()
+    for d in range(1, E):
+        pl.semaphore_signal(barrier, inc=1, device_id=column(d), device_id_type=MESH)
+    pl.semaphore_signal(barrier, inc=1, device_id=partner, device_id_type=MESH)
+
+    @pl.when(has_low)
+    def _():
+        pl.semaphore_signal(barrier, inc=1, device_id=below, device_id_type=MESH)
+
+    @pl.when(has_high)
+    def _():
+        pl.semaphore_signal(barrier, inc=1, device_id=above, device_id_type=MESH)
+
+    arrays = (
+        (tokens_in, tokens), (expert_gain_in, expert_gain), (routes_in, routes),
+        (scores_in, scores), (key_in, key), (value_in, value), (key_gain_in, key_gain),
+        (query_in, query), (query_gain_in, query_gain), (offset_in, offset),
+    )
+    loads = [pltpu.make_async_copy(src, dst, in_sem.at[i]) for i, (src, dst) in enumerate(arrays)]
+    for load in loads:
+        load.start()
     local = [
         pltpu.make_async_copy(src, dst.at[0], lw_sem.at[i])
         for i, (src, dst) in enumerate(((gate, wg), (up, wu), (down, wd), (mixer, wm)))
     ]
     for copy in local:
         copy.start()
-    barrier = pltpu.get_barrier_semaphore()
-    for d in range(1, E):
-        pl.semaphore_signal(barrier, inc=1, device_id=column(d), device_id_type=MESH)
-    pl.semaphore_signal(barrier, inc=1, device_id=partner, device_id_type=MESH)
-
-    @pl.when(has_low)
-    def _():
-        pl.semaphore_signal(barrier, inc=1, device_id=below, device_id_type=MESH)
-
-    @pl.when(has_high)
-    def _():
-        pl.semaphore_signal(barrier, inc=1, device_id=above, device_id_type=MESH)
+    for load in loads[:4]:
+        load.wait()
 
     x = tokens[...].astype(F32)
     x = x * lax.rsqrt(jnp.mean(x * x, axis=1, keepdims=True) + EPS) * expert_gain[...]
@@ -114,24 +128,23 @@
     s0, s1 = scores[0:1], scores[1:2]
     w0 = 1.0 / (1.0 + jnp.exp(s1 - s0))
     w1 = 1.0 / (1.0 + jnp.exp(s0 - s1))
-    pieces = [route[0:1], route[1:2]]
-    for p0, p1 in zip(split3(w0), split3(w1)):
-        pieces += [p0.astype(F32), p1.astype(F32)]
     line = lax.broadcasted_iota(jnp.int32, (TAGS, C), 0)
-    tags = jnp.zeros((TAGS, C), F32)
-    for i, piece in enumerate(pieces):
-        tags = jnp.where(line == i, piece, tags)
-    tags = tags.T
-    xb[z, :, :B] = normed[:, A:]
-    xb[z, :, B:] = tags.astype(BF16)
+    label = jnp.zeros((TAGS, C), F32)
+    for i, piece in enumerate((route[0:1], route[1:2], w0, w1)):
+        label = jnp.where(line == i, piece, label)
+    tg[z] = label
+    xb[z] = normed[:, A:]
+
+    def fwd_t(l, sems, dev):
+        return rcopy(tg.at[l], tg.at[l], sems.at[l], ft_recv.at[l], dev)
 
     def fwd_b(l, j, sems, dev):
         s = pl.ds(j * TB, TB)
-        return rcopy(xb.at[l, s], xb.at[l, s], sems.at[l, j], fb_recv.at[l, j], dev)
+        return rcopy(xb.at[l, s], xb.at[l, s], sems.at[l], fb_recv.at[l, j], dev)
 
     def fwd_a(l, j, sems, dev):
         s = pl.ds(j * R, R)
-        return rcopy(xa.at[l, s], xa.at[l, s], sems.at[l, j], fa_recv.at[l, j], dev)
+        return rcopy(xa.at[l, s], xa.at[l, s], sems.at[l], fa_recv.at[l, j], dev)
 
     def both_ways(make, chunks, up_sems, dn_sems):
         for j in range(chunks):
@@ -153,15 +166,14 @@
     slot_expert = jnp.bitwise_xor(lax.shift_right_logical(slot, shift), ep).astype(F32)
     slot_rank = jnp.bitwise_and(slot, cap - 1).astype(F32)
 
-    def selection(l, t):
+    def selection(l):
+        t = jnp.concatenate([tg[l], jnp.zeros((C - TAGS, C), F32)], axis=0).T
         m0 = t[:, 0:1] == slot_expert
         m1 = t[:, 1:2] == slot_expert
         member = jnp.where(jnp.logical_or(m0, m1), 1.0, 0.0)
         rank = dot(before, member.astype(BF16))
         chosen = jnp.where(rank == slot_rank, member, 0.0)
-        v0 = t[:, 2:3] + t[:, 4:5] + t[:, 6:7]
-        v1 = t[:, 3:4] + t[:, 5:6] + t[:, 7:8]
-        weight = chosen * jnp.where(m0, v0, v1)
+        weight = chosen * jnp.where(m0, t[:, 2:3], t[:, 3:4])
         high = weight.astype(BF16)
         wh[l] = high
         wl[l] = (weight - high.astype(F32)).astype(BF16)
@@ -176,22 +188,23 @@
         return rcopy(src.at[s], dst.at[s], send, recv, column(1))
 
     def dispatch_b(l, chosen):
-        out = dot(chosen, xb[l, :, :B]).astype(BF16)
+        out = dot(chosen, xb[l]).astype(BF16)
         xbs[l, :cap] = out[:cap]
         ob[l, cap:] = out[cap:]
         for d in range(1, E):
             plane(ob.at[l], xbs.at[l], pb_send.at[l], pb_recv.at[l], d).start()
 
-    chosen = selection(z, tags)
+    chosen = selection(z)
     out = dot(chosen, normed[:, :A]).astype(BF16)
     xa[z, :cap] = out[:cap]
     oa[cap:] = out[cap:]
     with jax.named_scope("barrier"):
      pl.semaphore_wait(barrier, E + has_low.astype(jnp.int32) + has_high.astype(jnp.int32))
 
+    both_ways(lambda l, j, sems, dev: fwd_t(l, sems, dev), 1, ft_up, ft_dn)
     both_ways(fwd_b, B_CHUNKS, fb_up, fb_dn)
     for d in range(1, E):
-        plane(oa, xa.at[z], pa_send, pa_recv, d).start()
+        plane(oa, xa.at[z], pa_send, pa_recv.at[d], d).start()
 
     swaps = [
         rcopy(src, dst.at[1], pw_send.at[i], pw_recv.at[i], partner)
@@ -202,9 +215,19 @@
 
     dispatch_b(z, chosen)
 
-    with jax.named_scope("w_own_a"):
-        rest(oa, xa.at[z], pa_send, pa_recv).wait_recv()
-    both_ways(fwd_a, A_CHUNKS, fa_up, fa_dn)
+    for j in range(A_CHUNKS):
+        with jax.named_scope("w_own_a"):
+            for d in range(max(1, j * R // cap), (j + 1) * R // cap):
+                plane(oa, xa.at[z], pa_send, pa_recv.at[d], d).wait_recv()
+
+        @pl.when(has_high)
+        def _():
+            fwd_a(z, j, fa_up, above).start()
+
+        @pl.when(has_low)
+        def _():
+            fwd_a(z, j, fa_dn, below).start()
+
 
     def on_sides(t, work):
         @pl.when(z - t >= 0)
@@ -217,6 +240,13 @@
 
     def arrive_b(l, onward, side):
         sems, dev = ((fb_up, above), (fb_dn, below))[side]
+        tags = fwd_t(l, (ft_up, ft_dn)[side], dev)
+        tags.wait_recv()
+
+        @pl.when(onward)
+        def _():
+            tags.start()
+
         for j in range(B_CHUNKS):
             with jax.named_scope("w_fwd_b"):
                 fwd_b(l, j, sems, dev).wait_recv()
@@ -226,7 +256,7 @@
                 fwd_b(l, j, sems, dev).start()
 
         with jax.named_scope("dispatch"):
-            dispatch_b(l, selection(l, xb[l, :, B:].astype(F32)))
+            dispatch_b(l, selection(l))
 
     def arrive_a(l, onward, side):
         sems, dev = ((fa_up, above), (fa_dn, below))[side]
@@ -242,6 +272,8 @@
 
     heads = key.shape[1] // HEAD_DIM
     aw = key.shape[1]
+    for load in loads[4:7]:
+        load.wait()
     kv[:C, :aw] = jnp.concatenate(norm_heads(key, key_gain[...]), axis=1)
     kv[:C, aw:] = value[...]
 
@@ -256,6 +288,8 @@
          for d in range(1, E):
             kv_copy(d).wait_recv()
         length = E * C
+        for load in loads[7:]:
+            load.wait()
         query_norm = norm_heads(query, query_gain[...])
         lane = lax.broadcasted_iota(jnp.int32, (C, length), 1)
         bits = C.bit_length() - 1
@@ -267,7 +301,7 @@
         for h in range(heads):
             part = slice(h * HEAD_DIM, (h + 1) * HEAD_DIM)
             vpart = slice(aw + h * HEAD_DIM, aw + (h + 1) * HEAD_DIM)
-            s = dot_t(query_norm[h], kv[:, part]) * HEAD_DIM ** (-0.5) + offset[h]
+            s = dot_t(query_norm[h], kv[:, part]) * HEAD_DIM ** (-0.5) + offset[:, h : h + 1]
             soft = jnp.log1p(jnp.exp(-jnp.abs(s)))
             rise = jnp.minimum(s, 0.0) - soft
             fail = jnp.where(allowed, jnp.minimum(-s, 0.0) - soft, 0.0)
@@ -331,23 +365,23 @@
         qb[l, :cap] = pb[l, :cap]
 
     def ret_a(l, j, buf, recv, dev):
-        s = pl.ds(j * R, R)
-        return rcopy(pa.at[l, s], buf.at[l, s], za_send.at[l, j], recv.at[l, j], dev)
+        s = pl.ds(j * RR, RR)
+        return rcopy(pa.at[l, s], buf.at[l, s], za_send.at[l], recv.at[l, j], dev)
 
     def ret_b(l, j, buf, recv, dev):
         s = pl.ds(j * TR, TR)
-        return rcopy(mb.at[l, s], buf.at[l, s], zb_send.at[l, j], recv.at[l, j], dev)
+        return rcopy(mb.at[l, s], buf.at[l, s], zb_send.at[l], recv.at[l, j], dev)
 
     def ret_m(l, buf, recv, dev):
         return rcopy(ms.at[l], buf.at[l], zm_send.at[l], recv.at[l], dev)
 
-    def mix(l, s):
-        return dot(wh[l, s], qb[l]) + dot(wl[l, s], qb[l])
+    def mix(l, rows):
+        return dot(wh[l], rows) + dot(wl[l], rows)
 
     def returns_a(l, incoming, side):
         buf, recv, dev = ((ral, za_low, above), (rah, za_high, below))[side]
-        for j in range(A_CHUNKS):
-            s = pl.ds(j * R, R)
+        for j in range(A_BACK):
+            s = pl.ds(j * RR, RR)
 
             @pl.when(incoming)
             def _():
@@ -371,17 +405,17 @@
         buf, recv, dev = ((rbl, zb_low, above), (rbh, zb_high, below))[side]
         with jax.named_scope("w_ret_plane"):
             rest(pb.at[l], qb.at[l], rb_send.at[l], rb_recv.at[l]).wait_recv()
+        acc[...] = mix(l, qb[l])
         for j in range(B_BACK):
             s = pl.ds(j * TR, TR)
-            acc[...] = mix(l, s)
 
             @pl.when(incoming)
             def _():
                 with jax.named_scope("w_ret_b"):
                     ret_b(l, j, buf, recv, dev).wait_recv()
-                acc[...] = acc[...] + buf[l, s].astype(F32)
-
-            mb[l, s] = acc[...].astype(BF16)
+                acc[s] = acc[s] + buf[l, s].astype(F32)
+
+            mb[l, s] = acc[s].astype(BF16)
             ret_b(l, j, buf, recv, dev).start()
 
     def on_targets(t, work):
@@ -430,11 +464,11 @@
         def _():
             on_sides(t + 1, arrive_b)
 
-        @pl.when(t > 0)
+        @pl.when(t == Z - 1)
         def _():
             levels_of(t, send_home)
 
-        @pl.when(t == Z - 1)
+        @pl.when(jnp.logical_and(t == Z - 1, jnp.logical_not(at_end)))
         def _():
             send_home(z)
 
@@ -450,6 +484,10 @@
         @pl.when(t < Z - 1)
         def _():
             on_sides(t + 1, arrive_a)
+
+        @pl.when(jnp.logical_and(t > 0, t < Z - 1))
+        def _():
+            levels_of(t, send_home)
 
         @pl.when(t == 1)
         def _():
@@ -479,29 +517,45 @@
             on_targets(t, returns_b)
         return carry
 
-    lax.fori_loop(Z, 2 * Z - 1, tail_a, 0)
-    lax.fori_loop(Z - 1, 2 * Z - 1, tail_b, 0)
-
-    for j in range(A_CHUNKS):
-        s = pl.ds(j * R, R)
-
-        @pl.when(has_low)
-        def _():
-            with jax.named_scope("f_a_low"):
-             ret_a(z, j, ral, za_low, above).wait_recv()
-            pa[z, s] = (pa[z, s].astype(F32) + ral[z, s].astype(F32)).astype(BF16)
-
-        @pl.when(has_high)
-        def _():
-            with jax.named_scope("f_a_high"):
-             ret_a(z, j, rah, za_high, below).wait_recv()
-            pa[z, s] = (pa[z, s].astype(F32) + rah[z, s].astype(F32)).astype(BF16)
-
-        fa[s] = pa[z, s]
-        if j == 0:
-            qa[:cap] = pa[z, :cap]
-        for d in range(max(1, j * R // cap), (j + 1) * R // cap):
-            plane(fa, qa, ra_send, ra_recv, d).start()
+    def own_a():
+        for j in range(A_BACK):
+            s = pl.ds(j * RR, RR)
+
+            @pl.when(has_low)
+            def _():
+                with jax.named_scope("f_a_low"):
+                 ret_a(z, j, ral, za_low, above).wait_recv()
+                pa[z, s] = (pa[z, s].astype(F32) + ral[z, s].astype(F32)).astype(BF16)
+
+            @pl.when(has_high)
+            def _():
+                with jax.named_scope("f_a_high"):
+                 ret_a(z, j, rah, za_high, below).wait_recv()
+                pa[z, s] = (pa[z, s].astype(F32) + rah[z, s].astype(F32)).astype(BF16)
+
+            fa[s] = pa[z, s]
+            if (j + 1) * RR == max(cap, RR):
+                qa[:cap] = pa[z, :cap]
+            for d in range(max(1, j * RR // cap), (j + 1) * RR // cap):
+                plane(fa, qa, ra_send, ra_recv, d).start()
+
+    def tail(t, carry):
+        tail_a(t, carry)
+
+        @pl.when(jnp.logical_and(t == 2 * Z - 2, jnp.logical_not(at_end)))
+        def _():
+            own_a()
+
+        tail_b(t - 1, carry)
+        return carry
+
+    lax.fori_loop(Z, 2 * Z, tail, 0)
+
+    @pl.when(at_end)
+    def _():
+        send_home(z)
+        own_a()
+
 
     total = ms[z].astype(F32)
     att_out[...] = total.astype(BF16)
@@ -518,29 +572,8 @@
         att_out[...] = (att_out[...].astype(F32) + rmh[z].astype(F32)).astype(BF16)
 
     rest(pb.at[z], qb.at[z], rb_send.at[z], rb_recv.at[z]).wait_recv()
-    for j in range(B_BACK):
-        s = pl.ds(j * TR, TR)
-        acc[...] = mix(z, s)
-
-        @pl.when(has_low)
-        def _():
-            with jax.named_scope("f_b_low"):
-             ret_b(z, j, rbl, zb_low, above).wait_recv()
-            acc[...] = acc[...] + rbl[z, s].astype(F32)
-
-        @pl.when(has_high)
-        def _():
-            with jax.named_scope("f_b_high"):
-             ret_b(z, j, rbh, zb_high, below).wait_recv()
-            acc[...] = acc[...] + rbh[z, s].astype(F32)
-
-        exp_out[s, A:] = acc[...].astype(BF16)
-
-    with jax.named_scope("f_plane_a"):
-     rest(fa, qa, ra_send, ra_recv).wait_recv()
-    exp_out[:, :A] = (dot(wh[z], qa[...]) + dot(wl[z], qa[...])).astype(BF16)
-
-    rest(oa, xa.at[z], pa_send, pa_recv).wait_send()
+    acc[...] = mix(z, qb[z])
+    rest(oa, xa.at[z], pa_send, pa_recv.at[1]).wait_send()
     rest(fa, qa, ra_send, ra_recv).wait_send()
     hm_copy.wait_send()
     for swap in swaps:
@@ -554,30 +587,47 @@
 
         @pl.when(jnp.logical_and(l <= z, has_high))
         def _():
-            for j in range(B_CHUNKS):
-                fwd_b(l, j, fb_up, above).wait_send()
-            for j in range(A_CHUNKS):
-                fwd_a(l, j, fa_up, above).wait_send()
+            fwd_t(l, ft_up, above).wait_send()
+            rcopy(xb.at[l], xb.at[l], fb_up.at[l], fb_recv.at[l, 0], above).wait_send()
+            rcopy(xa.at[l], xa.at[l], fa_up.at[l], fa_recv.at[l, 0], above).wait_send()
 
         @pl.when(jnp.logical_and(l >= z, has_low))
         def _():
-            for j in range(B_CHUNKS):
-                fwd_b(l, j, fb_dn, below).wait_send()
-            for j in range(A_CHUNKS):
-                fwd_a(l, j, fa_dn, below).wait_send()
+            fwd_t(l, ft_dn, below).wait_send()
+            rcopy(xb.at[l], xb.at[l], fb_dn.at[l], fb_recv.at[l, 0], below).wait_send()
+            rcopy(xa.at[l], xa.at[l], fa_dn.at[l], fa_recv.at[l, 0], below).wait_send()
 
         @pl.when(l != z)
         def _():
-            for j in range(A_CHUNKS):
-                ret_a(l, j, ral, za_low, above).wait_send()
-            for j in range(B_BACK):
-                ret_b(l, j, rbl, zb_low, above).wait_send()
+            rcopy(pa.at[l], ral.at[l], za_send.at[l], za_low.at[l, 0], above).wait_send()
+            rcopy(mb.at[l], rbl.at[l], zb_send.at[l], zb_low.at[l, 0], above).wait_send()
             ret_m(l, rml, zm_low, above).wait_send()
 
         return carry
 
-    lax.fori_loop(0, Z, drain, 0)
-
+    with jax.named_scope("drain"):
+        lax.fori_loop(0, Z, drain, 0)
+
+    for j in range(B_BACK):
+        s = pl.ds(j * TR, TR)
+
+        @pl.when(has_low)
+        def _():
+            with jax.named_scope("f_b_low"):
+                ret_b(z, j, rbl, zb_low, above).wait_recv()
+            acc[s] = acc[s] + rbl[z, s].astype(F32)
+
+        @pl.when(has_high)
+        def _():
+            with jax.named_scope("f_b_high"):
+                ret_b(z, j, rbh, zb_high, below).wait_recv()
+            acc[s] = acc[s] + rbh[z, s].astype(F32)
+
+        exp_out[s, A:] = acc[s].astype(BF16)
+
+    with jax.named_scope("f_plane_a"):
+        rest(fa, qa, ra_send, ra_recv).wait_recv()
+    exp_out[:, :A] = mix(z, qa[...]).astype(BF16)
 
 def layer(
     query, key, value, query_gain, key_gain, offset, mixer, tokens, expert_gain, routes, scores,
@@ -595,26 +645,34 @@
     rows = C // (2 * Z)
     dma = lambda *shape: pltpu.SemaphoreType.DMA(shape)
     vmem = pl.BlockSpec(memory_space=pltpu.VMEM)
-    smem = pl.BlockSpec(memory_space=pltpu.SMEM)
     hbm = pl.BlockSpec(memory_space=pl.ANY)
     kernel = functools.partial(body, E, Z, C, D, A)
     NA, NB = A_CHUNKS, B_CHUNKS
-    results = pl.pallas_call(
+    return pl.pallas_call(
         kernel,
         name="step",
-        out_shape=(
-            jax.ShapeDtypeStruct((rows, D), BF16),
-            jax.ShapeDtypeStruct((C, D), BF16),
-        ),
-        in_specs=[vmem, vmem, vmem, vmem, vmem, smem, hbm, vmem, vmem, vmem, vmem, hbm, hbm, hbm],
+        out_shape=(pltpu.VMEM((rows, D), BF16), pltpu.VMEM((C, D), BF16)),
+        in_specs=[hbm] * 14,
         out_specs=(vmem, vmem),
         scratch_shapes=[
+            pltpu.VMEM((C, aw), BF16),
+            pltpu.VMEM((C, aw), BF16),
+            pltpu.VMEM((C, aw), BF16),
+            pltpu.VMEM((1, HEAD_DIM), F32),
+            pltpu.VMEM((1, HEAD_DIM), F32),
+            pltpu.VMEM((1, aw // HEAD_DIM), F32),
+            pltpu.VMEM((C, D), BF16),
+            pltpu.VMEM((1, D), F32),
+            pltpu.VMEM((TOP_K, C), jnp.int32),
+            pltpu.VMEM((TOP_K, C), F32),
+            dma(10),
             pltpu.VMEM((2, H, D), BF16),
             pltpu.VMEM((2, H, D), BF16),
             pltpu.VMEM((2, H, D), BF16),
             pltpu.VMEM((2, aw, D), BF16),
             pltpu.VMEM((C, D), BF16),
-            pltpu.VMEM((Z, C, B + TAGS), BF16),
+            pltpu.VMEM((Z, TAGS, C), F32),
+            pltpu.VMEM((Z, C, B), BF16),
             pltpu.VMEM((Z, slots, A), BF16),
             pltpu.VMEM((Z, slots, B), BF16),
             pltpu.VMEM((slots, A), BF16),
@@ -631,7 +689,7 @@
             pltpu.VMEM((Z, C, B), BF16),
             pltpu.VMEM((Z, C, B), BF16),
             pltpu.VMEM((slots, A), BF16),
-            pltpu.VMEM((C // B_BACK, B), F32),
+            pltpu.VMEM((C, B), F32),
             pltpu.VMEM((E * C, 2 * aw), BF16),
             pltpu.VMEM((Z, 2, rows, aw), F32),
             pltpu.VMEM((Z, rows, aw), F32),
@@ -639,44 +697,25 @@
             pltpu.VMEM((Z, rows, D), BF16),
             pltpu.VMEM((Z, rows, D), BF16),
             dma(4), dma(4), dma(4), dma(2),
-            pltpu.SemaphoreType.DMA, pltpu.SemaphoreType.DMA,
+            pltpu.SemaphoreType.DMA, dma(E),
             dma(E), dma(E),
             dma(Z), dma(Z),
             dma(Z), dma(Z),
             pltpu.SemaphoreType.DMA, pltpu.SemaphoreType.DMA,
-            dma(Z, NB), dma(Z, NB), dma(Z, NB),
-            dma(Z, NA), dma(Z, NA), dma(Z, NA),
-            dma(Z, NA), dma(Z, NA), dma(Z, NA),
-            dma(Z, B_BACK), dma(Z, B_BACK), dma(Z, B_BACK),
+            dma(Z), dma(Z), dma(Z),
+            dma(Z), dma(Z), dma(Z, NB),
+            dma(Z), dma(Z), dma(Z, NA),
+            dma(Z), dma(Z, A_BACK), dma(Z, A_BACK),
+            dma(Z), dma(Z, B_BACK), dma(Z, B_BACK),
             dma(Z), dma(Z), dma(Z),
         ],
         compiler_params=pltpu.CompilerParams(
             collective_id=0, has_side_effects=True, vmem_limit_bytes=62 * 1024 * 1024
         ),
     )(
-        query, key, value, query_gain[None], key_gain[None], offset, mixer, tokens,
+        query, key, value, query_gain[None], key_gain[None], offset[None], mixer, tokens,
         expert_gain[None], routes.T, scores.T, gate[0].T, up[0].T, down[0],
     )
-    return pl.pallas_call(
-        hand_over,
-        name="hand_over",
-        out_shape=(
-            jax.ShapeDtypeStruct((rows, D), BF16),
-            jax.ShapeDtypeStruct((C, D), BF16),
-        ),
-        in_specs=[vmem, vmem],
-        out_specs=(hbm, hbm),
-        scratch_shapes=[dma(2)],
-    )(*results)
-
-
-def hand_over(att_in, exp_in, att_out, exp_out, sems):
-    first = pltpu.make_async_copy(att_in, att_out, sems.at[0])
-    second = pltpu.make_async_copy(exp_in, exp_out, sems.at[1])
-    second.start()
-    first.start()
-    second.wait()
-    first.wait()
 
 
 def solution(mesh):

time: 98.7 us -> 93.8 us (0.950)
  Pallas kernels: 97.9 us -> 91.6 us
  local copies, waits for them, and re-layouts: 0 us -> 1.42 us
    pallas_call x2 -> x1, Pallas kernels: 97.9 us -> 91.6 us  [layer(): pl.pallas_call(kernel, name='step', out_shape=(pltpu.VMEM((rows, D), BF16...]
    unnamed x0 -> x2, local copies, waits for them, and re-layouts: none -> 1.42 us
where the time goes in v2:
time: 93.8 us; the launch traced here: 93.7 us
  Pallas kernels  91.6 us (98%)
  local copies, waits for them, and re-layouts  1.42 us (2%)
    pallas_call x1, Pallas kernels, layer(): pl.pallas_call(kernel, name='step', out_shape=(pltpu.VMEM((rows, D), BF16...  91.6 us

profile of v2, /device:TPU:0, one launch (start us, length us, event | category | flops | bytes accessed | tf_op | source)
XLA Modules:
  0.0 93.7 jit_solution(2364337533381988525)
XLA Ops:
  0.6 91.6 %step.1 = (bf16[16,2048]{1,0:T(8,128)(2,1)S(1)}, bf16[128,2048]{1,0:T(8,128)(2,1)S(1)}) custom-call(bf16[128,256]{1,0:T(8,128)(2,1)} %query_in.1, bf16[128,256]{1,0:T(8,128)(2,1)} %key_in.1, bf16[128,256]{1,0:T(8,128)(2,1)} %value_in.1, f32[1,64]{1,0:T(1,128)} %bitcast.19, f32[1,64]{1,0:T(1,128)} %bitcast.20, f32[1,4]{1,0:T(1,128)} %bitcast.21, ...), custom_call_target="tpu_custom_call" | custom-call | tf_op jit(solution)/shard_map/step/pallas_call | solution.py:651
  92.3 0.6 copy.18
  92.9 0.8 copy.19
